TPU v7x, 32 devices: a whole 2x2x4 slice. The times are simulated.
32 devices in a mesh: sp: 8 (over z, x), tp: 4 (over y, core).
Axes of the slice: x: 2, y: 2, z: 4, core: 2. Of those that a mesh axis runs over, the one named last changes fastest.
Arguments:
- residual: bfloat16 [6144, 2048], P('sp'), may hold values from -6 to 6
- query_matrix: bfloat16 [6144, 1024], P('sp', 'tp'), may hold values from -6 to 6
- key_matrix: bfloat16 [6144, 1024], P('sp', 'tp'), may hold values from -6 to 6
- value_matrix: bfloat16 [6144, 2048], P('sp', 'tp'), may hold values from -6 to 6
- output_gate_logit: bfloat16 [6144, 2048], P('sp', 'tp'), may hold values from -6 to 6
- input_gate_log: float32 [6144, 8], P('sp', 'tp'), may hold values from -4 to 125
- forget_gate_logit: float32 [6144, 8], P('sp', 'tp')
- extra_head_decay: float32 [6144, 8], P('sp', 'tp'), may hold values from -1 to 0
- head_norm_gain: float32 [2048], P('tp'), may hold values from 0.1 to 1.9
- projection: bfloat16 [2048, 2048], P('tp'), may hold values from -5.303301 to 5.303301
- cell_output_gain: float32 [2048], replicated, may hold values from 0.1 to 1.9
- mixer_input_gain: float32 [2048], replicated, may hold values from 0.1 to 1.9
- mixer_gate_weight: bfloat16 [2048, 5120], P('sp', 'tp'), may hold values from -0.125 to 0.125
- mixer_up_weight: bfloat16 [2048, 5120], P('sp', 'tp'), may hold values from -0.125 to 0.125
- mixer_down_weight: bfloat16 [5120, 2048], P('tp', 'sp'), may hold values from -0.078125 to 0.078125
Outputs:
- updated: bfloat16 [6144, 2048], P('sp', 'tp')
All inputs are finite; a program needn't handle non-finite values.
Results may differ from a plain program's by a relative error of at most 0.014.
Values may be sent and summed in bfloat16 or wider, within the bound.
A program may use at most 128 MiB of HBM per device.

v0:
```python
import jax
import jax.numpy as jnp
from jax import lax
from jax.sharding import PartitionSpec as P

DQK = 128
DV = 256
HIGHEST = lax.Precision.HIGHEST
EPSILON = 1e-06
LOWEST_LOG = -1e30


def carried_in(value, axis, join, neutral):
    count, mine = (lax.axis_size(axis), lax.axis_index(axis))
    pieces = jax.tree.map(lambda part: lax.all_gather(part, axis), value)
    subtotal = jax.tree.map(
        lambda part, zero: jnp.full_like(part, 0) + jnp.asarray(zero, part.dtype), value, neutral
    )

    def turn(position, subtotal):
        longer = join(subtotal, jax.tree.map(lambda part: part[position], pieces))
        return jax.tree.map(lambda new, old: jnp.where(position < mine, new, old), longer, subtotal)

    return lax.fori_loop(0, count - 1, turn, subtotal)


def heads_first(array, heads, width):
    return array.reshape(array.shape[0], heads, width).transpose(1, 0, 2)


def read_out(
    query_low, key_low, value_low, in_logs, running_log_total, memory, normalizer, stabilizer
):
    length = query_low.shape[1]
    causal = lax.broadcasted_iota(jnp.int32, (length, length), 0) >= lax.broadcasted_iota(
        jnp.int32, (length, length), 1
    )
    spread = running_log_total[:, :, None] - running_log_total[:, None, :] + in_logs[:, None, :]
    spread = jnp.where(causal[None], spread, -jnp.inf)
    carried = running_log_total + stabilizer[:, None]
    running = jnp.maximum(carried, jnp.max(spread, axis=-1))
    scores = jnp.einsum(
        "htd,hsd->hts", query_low, key_low, preferred_element_type=jnp.float32
    ) * DQK ** (-0.5)
    weights = jnp.exp(spread - running[:, :, None]) * scores
    scaled = jnp.exp(carried - running)
    scaled_query = query_low.astype(jnp.float32) * DQK ** (-0.5)
    numerator = jnp.einsum(
        "hts,hsv->htv", weights.astype(jnp.bfloat16), value_low, preferred_element_type=jnp.float32
    )
    numerator = numerator + scaled[:, :, None] * jnp.einsum(
        "hvd,htd->htv", memory, scaled_query, precision=HIGHEST
    )
    denominator = jnp.sum(weights, axis=-1) + scaled * jnp.einsum(
        "hd,htd->ht", normalizer, scaled_query, precision=HIGHEST
    )
    return numerator / jnp.maximum(jnp.abs(denominator), jnp.exp(-running))[:, :, None]


def fold_state(keyed, valued, in_logs, running_log_total, memory, normalizer, stabilizer):
    last = running_log_total[:, -1]
    lifted = last[:, None] - running_log_total + in_logs
    new_max = jnp.maximum(last + stabilizer, jnp.max(lifted, axis=-1))
    weights = jnp.exp(lifted - new_max[:, None])
    retained = jnp.exp(last + stabilizer - new_max)
    memory = retained[:, None, None] * memory + jnp.einsum(
        "hsv,hsd->hvd", weights[:, :, None] * valued, keyed, precision=HIGHEST
    )
    normalizer = retained[:, None] * normalizer + jnp.einsum(
        "hs,hsd->hd", weights, keyed, precision=HIGHEST
    )
    return (memory, normalizer, new_max)


def join_states(earlier, later):
    early_decay, early_memory, early_normalizer, early_max = earlier
    late_decay, late_memory, late_normalizer, late_max = later
    joined_max = jnp.maximum(late_decay + early_max, late_max)
    first_scale = jnp.exp(late_decay + early_max - joined_max)
    second_scale = jnp.exp(late_max - joined_max)
    memory = first_scale[:, None, None] * early_memory + second_scale[:, None, None] * late_memory
    normalizer = first_scale[:, None] * early_normalizer + second_scale[:, None] * late_normalizer
    return (early_decay + late_decay, memory, normalizer, joined_max)


def body(
    residual,
    query_matrix,
    key_matrix,
    value_matrix,
    output_gate_logit,
    input_gate_log,
    forget_gate_logit,
    extra_head_decay,
    head_norm_gain,
    projection,
    cell_output_gain,
    mixer_input_gain,
    mixer_gate_weight,
    mixer_up_weight,
    mixer_down_weight,
):
    tok_rows = residual.shape[0]
    width = residual.shape[1]
    heads_here = input_gate_log.shape[1]
    query_low = heads_first(query_matrix, heads_here, DQK)
    key_low = heads_first(key_matrix, heads_here, DQK)
    value_low = heads_first(value_matrix, heads_here, DV)
    keyed = key_low.astype(jnp.float32)
    valued = value_low.astype(jnp.float32)
    in_logs = input_gate_log.T
    running_log_total = jnp.cumsum(
        (jax.nn.log_sigmoid(forget_gate_logit) + extra_head_decay).T, axis=-1
    )
    zero_memory = jnp.zeros((heads_here, DV, DQK), jnp.float32)
    zero_normalizer = jnp.zeros((heads_here, DQK), jnp.float32)
    lowest = jnp.full((heads_here,), LOWEST_LOG, jnp.float32)
    local_memory, local_normalizer, local_max = fold_state(
        keyed, valued, in_logs, running_log_total, zero_memory, zero_normalizer, lowest
    )
    prior_decay, prior_memory, prior_normalizer, prior_max = carried_in(
        (running_log_total[:, -1], local_memory, local_normalizer, local_max),
        "sp",
        join_states,
        (jnp.zeros_like(lowest), zero_memory, zero_normalizer, lowest),
    )
    start_max = jnp.maximum(prior_decay, prior_max)
    lift = jnp.exp(prior_max - start_max)
    cells = read_out(
        query_low,
        key_low,
        value_low,
        in_logs,
        running_log_total,
        lift[:, None, None] * prior_memory,
        lift[:, None] * prior_normalizer,
        start_max,
    )
    centered = cells - jnp.mean(cells, axis=-1, keepdims=True)
    normed = centered * lax.rsqrt(jnp.mean(centered * centered, axis=-1, keepdims=True) + EPSILON)
    normed = normed * head_norm_gain.reshape(heads_here, DV)[:, None, :]
    normed = normed.transpose(1, 0, 2).reshape(tok_rows, heads_here * DV)
    gated = (normed * jax.nn.sigmoid(output_gate_logit.astype(jnp.float32))).astype(jnp.bfloat16)
    cols_here = width // lax.axis_size("tp")
    offset = lax.axis_index("tp") * cols_here
    columns = projection
    mixed = (
        lax.psum_scatter(
            lax.dot_general(
                columns, gated, (((0,), (1,)), ((), ())), preferred_element_type=jnp.float32
            ).astype(jnp.bfloat16),
            "tp",
            scatter_dimension=0,
            tiled=True,
        )
        .astype(jnp.float32)
        .T
    )
    squares = lax.psum(jnp.sum(mixed * mixed, axis=-1), "tp")
    mixed = (
        mixed
        * lax.rsqrt(squares / width + EPSILON)[:, None]
        * lax.dynamic_slice_in_dim(cell_output_gain, offset, cols_here, 0)
    )
    own_residual = lax.dynamic_slice_in_dim(residual, offset, cols_here, 1).astype(jnp.float32)
    first_sum = (own_residual + mixed).astype(jnp.bfloat16)
    own_first = lax.optimization_barrier(first_sum).astype(jnp.float32)
    first_total = lax.psum(jnp.sum(own_first * own_first, axis=-1), "tp")
    own_gain = lax.dynamic_slice_in_dim(mixer_input_gain, offset, cols_here, 0)
    normed_own = (own_first * lax.rsqrt(first_total / width + EPSILON)[:, None] * own_gain).astype(
        jnp.bfloat16
    )
    normed_rows = lax.all_gather(normed_own, "tp", axis=1, tiled=True)
    columns = normed_rows
    gate_value = jnp.dot(
        columns,
        lax.all_gather(mixer_gate_weight, "sp", axis=0, tiled=True),
        preferred_element_type=jnp.float32,
    )
    up_value = jnp.dot(
        columns,
        lax.all_gather(mixer_up_weight, "sp", axis=0, tiled=True),
        preferred_element_type=jnp.float32,
    )
    activated = (jax.nn.silu(gate_value) * up_value).astype(jnp.bfloat16)
    down_terms = jnp.dot(
        activated,
        lax.all_gather(mixer_down_weight, "sp", axis=1, tiled=True),
        preferred_element_type=jnp.float32,
    )
    channel_out = lax.psum_scatter(
        down_terms.astype(jnp.bfloat16), "tp", scatter_dimension=1, tiled=True
    ).astype(jnp.float32)
    return (own_first + 0.5 * channel_out).astype(jnp.bfloat16)


def solution(mesh):
    return jax.shard_map(
        body,
        mesh=mesh,
        in_specs=(
            P("sp", None),
            P("sp", "tp"),
            P("sp", "tp"),
            P("sp", "tp"),
            P("sp", "tp"),
            P("sp", "tp"),
            P("sp", "tp"),
            P("sp", "tp"),
            P("tp"),
            P("tp", None),
            P(),
            P(),
            P("sp", "tp"),
            P("sp", "tp"),
            P("tp", "sp"),
        ),
        out_specs=P("sp", "tp"),
        check_vma=False,
    )
```

profile of v0, /device:TPU:0, one launch (start us, length us, event | category | flops | bytes accessed | tf_op | source)
XLA Modules:
  0.0 489.8 jit_solution(3324282672585852311)
XLA Ops:
  9.9 1.4 copy.54
  11.4 2.8 fusion.32
  15.8 22.4 %all-gather.3 = f32[8,1,2]{2,1,0:T(1,128)S(1)} all-gather(f32[1,1,2]{2,1,0:T(1,128)S(1)} %fusion.59), channel_id=1, replica_groups=mesh['sp'=8,'tp'=4] {'sp'}, dimensions={0}, use_global_device_ids=true | all-gather | bytes 72 | tf_op jit(solution)/shard_map/all_gather | solution.py:15
  38.1 17.6 %all-reduce = f32[16]{0:T(128)S(1)} all-reduce(f32[16]{0:T(128)S(1)} %dynamic-update-slice), channel_id=2, replica_groups=mesh['sp'=8,'tp'=4] {'sp'}, use_global_device_ids=true, to_apply=%add | all-reduce | flops 16 | bytes 128
  56.2 18.9 %all-gather.4 = f32[8,2,128]{2,1,0:T(2,128)S(1)} all-gather(f32[1,2,128]{2,1,0:T(2,128)S(1)} %add_bitcast_fusion.1), channel_id=4, replica_groups=mesh['sp'=8,'tp'=4] {'sp'}, dimensions={0}, use_global_device_ids=true | all-gather | bytes 9216 | tf_op jit(solution)/shard_map/all_gather | solution.py:15
  76.4 8.3 %while.20 = (s32[]{:T(128)}, f32[2]{0:T(128)S(1)}, f32[2,256,128]{2,1,0:T(8,128)S(1)}, f32[2,128]{1,0:T(2,128)S(1)}, f32[2]{0:T(128)S(1)}, /*index=5*/s32[]{:T(1...) while((s32[]{:T(128)}, f32[2]{0:T(128)S(1)}, ...), condition=%wide.region_4.5_spmd.clone, body=%wide.region_3.4_spmd.clone.sunk | while | flops 328984 | bytes 789781 | solution.py:24
  76.4 1.1 fusion.90
  77.6 1.1 fusion.90
  78.8 1.1 fusion.90
  80.0 1.1 fusion.90
  81.2 1.1 fusion.90
  82.4 1.1 fusion.90
  84.8 3.0 fusion.10
  88.5 1.5 fusion.37
  90.1 2.4 fusion.69
  92.9 1.5 fusion.28
  94.4 3.1 copy.47
  97.5 4.9 fusion.9
  104.7 32.8 %reduce-scatter.3.cloned.1.call-done = bf16[512,768]{0,1:T(8,128)(2,1)} async-done(((bf16[2048,768]{0,1:T(8,128)(2,1)}), bf16[512,768]{0,1:T(8,128)(2,1)}) %reduce-scatter.3.cloned.1.call-update) | async-done | bytes 786448 | tf_op jit(solution)/shard_map/reduce_scatter | solution.py:148
  137.6 1.4 fusion.15
  138.9 5.8 %psum.14 = f32[768]{0:T(1024)S(1)} all-reduce(f32[768]{0:T(1024)S(1)} %fusion.15), channel_id=1, replica_groups=mesh['sp'=8,'tp'=4] {'tp'}, use_global_device_ids=true, to_apply=%region_11.12 | all-reduce | flops 768 | bytes 6144 | tf_op jit(solution)/shard_map/psum | solution.py:159
  144.7 1.7 fusion.19
  146.7 5.7 %psum.15 = f32[768]{0:T(1024)S(1)} all-reduce(f32[768]{0:T(1024)S(1)} %fusion.20), channel_id=1, replica_groups=mesh['sp'=8,'tp'=4] {'tp'}, use_global_device_ids=true, to_apply=%region_13.14 | all-reduce | flops 768 | bytes 6144 | tf_op jit(solution)/shard_map/psum | solution.py:168
  152.3 1.1 fusion.22
  154.9 70.8 %all-gather.13.cloned.1.call-done = bf16[2048,1280]{1,0:T(8,128)(2,1)} async-done(((bf16[256,1280]{1,0:T(8,128)(2,1)}), bf16[2048,1280]{1,0:T(8,128)(2,1)}) %all-gather.13.cloned.1.call-update) | async-done | bytes 5242896 | tf_op jit(solution)/shard_map/all_gather | solution.py:177
  225.7 28.1 %all-gather.11.cloned.1.call-done = bf16[768,2048]{1,0:T(8,128)(2,1)} async-done(((bf16[768,512]{1,0:T(8,128)(2,1)}), bf16[768,2048]{1,0:T(8,128)(2,1)}) %all-gather.11.cloned.1.call-update) | async-done | bytes 3145744 | tf_op jit(solution)/shard_map/all_gather | solution.py:173
  253.8 9.6 %fusion.72 = f32[768,1280]{1,0:T(8,128)} fusion(bf16[768,2048]{1,0:T(8,128)(2,1)} %all-gather.11.cloned.1.call-done, bf16[2048,1280]{1,0:T(8,128)(2,1)} %all-gather.13.cloned.1.call-done), kind=kOutput, calls=%fused_computation.118 | convolution fusion | flops 4026531840 | bytes 12320768 | tf_op jit(solution)/shard_map/dot_general | solution.py:175
  263.4 78.4 %all-gather.15.cloned.1.call-done = bf16[2048,1280]{1,0:T(8,128)(2,1)} async-done(((bf16[256,1280]{1,0:T(8,128)(2,1)}), bf16[2048,1280]{1,0:T(8,128)(2,1)}) %all-gather.15.cloned.1.call-update) | async-done | bytes 5242896 | tf_op jit(solution)/shard_map/all_gather | solution.py:182
  341.8 86.9 %all-gather.17.cloned.1.call-done = bf16[1280,2048]{1,0:T(8,128)(2,1)} async-done(((bf16[1280,256]{1,0:T(8,128)(2,1)}), bf16[1280,2048]{1,0:T(8,128)(2,1)}) %all-gather.17.cloned.1.call-update) | async-done | bytes 5242896 | tf_op jit(solution)/shard_map/all_gather | solution.py:188
  428.7 16.0 %convolution_convert_fusion.1 = bf16[768,2048]{1,0:T(8,128)(2,1)} fusion(bf16[1280,2048]{1,0:T(8,128)(2,1)} %all-gather.17.cloned.1.call-done, bf16[768,2048]{1,0:T(8,128)(2,1)} %all-gather.11.cloned.1.call-done, bf16[2048,1280]{1,0:T(8,128)(2,1)} %all-gather.15.cloned.1.call-done, f32[768,1280]{1,0:T(8,128)} %fusion.72), kind=kOutput, calls=%fused_computation.23 | convolution fusion | flops 8060534784 | bytes 20709376 | tf_op jit(solution)/shard_map/dot_general | solution.py:186
  444.7 36.1 %reduce-scatter.5.cloned.1.call-done = bf16[768,512]{1,0:T(8,128)(2,1)} async-done(((bf16[768,2048]{1,0:T(8,128)(2,1)}), bf16[768,512]{1,0:T(8,128)(2,1)}) %reduce-scatter.5.cloned.1.call-update) | async-done | bytes 786448 | tf_op jit(solution)/shard_map/reduce_scatter | solution.py:191
  480.7 2.2 fusion.23
  (96 shorter events, 13.1 us)
Async XLA Ops:
  6.5 91.0 %copy-start = (bf16[512,2048]{1,0:T(8,128)(2,1)S(1)}, bf16[512,2048]{1,0:T(8,128)(2,1)}, u32[]{:S(2)}) copy-start(bf16[512,2048]{1,0:T(8,128)(2,1)} %param.26) | copy-start | bytes 6291460
  6.5 7.8 %copy-start.8 = (u32[32]{0:T(128)S(1)}, u32[32]{0:T(128)}, u32[]{:S(2)}) copy-start(u32[32]{0:T(128)} %constant.77) | copy-start | bytes 388
  6.5 49.4 %copy-start.4 = (bf16[768,256]{1,0:T(8,128)(2,1)S(1)}, bf16[768,256]{1,0:T(8,128)(2,1)}, u32[]{:S(2)}) copy-start(bf16[768,256]{1,0:T(8,128)(2,1)} %param.19) | copy-start | bytes 1179652
  6.5 49.3 %copy-start.6 = (f32[512]{0:T(512)S(1)}, f32[512]{0:T(512)}, u32[]{:S(2)}) copy-start(f32[512]{0:T(512)} %param.25) | copy-start | bytes 6148
  6.5 69.8 %all-gather.19.cloned.1.call-start = ((), (), s32[]{:S(2)}) async-start(), calls=%async_computation.8 | async-start | bytes 2359296 | tf_op jit(solution)/shard_map/all_gather | solution.py:15
  7.5 67.9 %copy-start.5 = (f32[768,2]{0,1:T(2,128)S(1)}, f32[768,2]{0,1:T(2,128)}, u32[]{:S(2)}) copy-start(f32[768,2]{0,1:T(2,128)} %param.22) | copy-start | bytes 18436
  11.3 26.8 %copy-start.1 = (bf16[768,512]{0,1:T(8,128)(2,1)}, bf16[768,512]{0,1:T(8,128)(2,1)S(1)}, u32[]{:S(2)}) copy-start(bf16[768,512]{0,1:T(8,128)(2,1)S(1)} %copy.54) | copy-start | bytes 2359300
  14.3 123.3 %reduce-scatter.3.cloned.1.call-start = ((), (), s32[]{:S(2)}) async-start(), calls=%async_computation.2 | async-start | bytes 3932160 | tf_op jit(solution)/shard_map/reduce_scatter | solution.py:148
  75.4 9.4 %copy-start.3 = (bf16[768,256]{1,0:T(8,128)(2,1)S(1)}, bf16[768,256]{1,0:T(8,128)(2,1)}, u32[]{:S(2)}) copy-start(bf16[768,256]{1,0:T(8,128)(2,1)} %param.18) | copy-start | bytes 1179652
  87.7 2.4 copy-start.2
  94.4 3.1 copy-start.7
  102.4 123.3 %all-gather.13.cloned.1.call-start = ((), (), s32[]{:S(2)}) async-start(), calls=%async_computation.4 | async-start | bytes 5898240 | tf_op jit(solution)/shard_map/all_gather | solution.py:177
  103.2 150.7 %all-gather.11.cloned.1.call-start = ((), (), s32[]{:S(2)}) async-start(), calls=%async_computation.3 | async-start | bytes 3932160 | tf_op jit(solution)/shard_map/all_gather | solution.py:173
  153.5 188.3 %all-gather.15.cloned.1.call-start = ((), (), s32[]{:S(2)}) async-start(), calls=%async_computation.5 | async-start | bytes 5898240 | tf_op jit(solution)/shard_map/all_gather | solution.py:182
  154.1 274.6 %all-gather.17.cloned.1.call-start = ((), (), s32[]{:S(2)}) async-start(), calls=%async_computation.6 | async-start | bytes 5898240 | tf_op jit(solution)/shard_map/all_gather | solution.py:188
  154.7 326.0 %reduce-scatter.5.cloned.1.call-start = ((), (), s32[]{:S(2)}) async-start(), calls=%async_computation.7 | async-start | bytes 3932160 | tf_op jit(solution)/shard_map/reduce_scatter | solution.py:191
Sparse Core Ops, SparseCore 0:
  14.4 52.0 all-gather.18
  102.5 34.9 reduce-scatter.2
  139.8 85.8 all-gather.12
  227.1 26.6 all-gather.10
  255.9 85.8 all-gather.14
  343.7 84.9 all-gather.16
  444.8 35.8 reduce-scatter.4
where the time goes:
time: 491 us; the launch traced here: 490 us
  waiting for transfers between devices  335 us (68%)
  blocking collectives  70.3 us (14%)
  matrix products  41 us (8%)
  other arithmetic  21.3 us (4%)
  between operations  14.3 us (3%)
  local copies, waits for them, and re-layouts  7.45 us (2%)
    all_gather x1, waiting for transfers between devices, body(): lax.all_gather(mixer_down_weight, 'sp', axis=1, tiled=True)  86.9 us
    all_gather x1, waiting for transfers between devices, body(): lax.all_gather(mixer_up_weight, 'sp', axis=0, tiled=True)  78.4 us
    all_gather x1, waiting for transfers between devices, body(): lax.all_gather(mixer_gate_weight, 'sp', axis=0, tiled=True)  70.8 us
    all_gather x2, blocking collectives, carried_in(): pieces = jax.tree.map(lambda part: lax.all_gather(part, axis), value)  41.3 us
    reduce_scatter x1, waiting for transfers between devices, body(): lax.psum_scatter(down_terms.astype(jnp.bfloat16), 'tp', scatter_dimension...  36.1 us
    reduce_scatter x1, waiting for transfers between devices, body(): lax.psum_scatter(lax.dot_general(columns, gated, (((0,), (1,)), ((), ()))...  32.8 us
    all_gather x1, waiting for transfers between devices, body(): normed_rows = lax.all_gather(normed_own, 'tp', axis=1, tiled=True)  28.1 us
    unnamed x1, blocking collectives  17.6 us
  transfers between devices with their start and end apart: 7, of which 6 were waited for; matrix products, arithmetic and copies ran while one was open for 4% of the time, Pallas kernels for 0%

commit v1 on v0

--- a/solution.py
+++ b/solution.py
@@ -170,7 +170,20 @@
     normed_own = (own_first * lax.rsqrt(first_total / width + EPSILON)[:, None] * own_gain).astype(
         jnp.bfloat16
     )
-    normed_rows = lax.all_gather(normed_own, "tp", axis=1, tiled=True)
+
+    def _tell_sector(x_local):
+        extent = jax.lax.axis_size("tp")
+        block_last = sorted(((p, (p + 1) % extent) for p in range(extent)))
+        small = x_local
+        inbox = [small]
+        for hop_no in [*range(1, extent)]:
+            small = jax.lax.ppermute(small, axis_name="tp", perm=block_last)
+            inbox.insert(0, small)
+        x_now = jnp.concatenate(inbox, axis=1)
+        value_now = jax.lax.axis_index("tp")
+        return jnp.roll(x_now, shift=(value_now + 1) * x_local.shape[1], axis=1)
+
+    normed_rows = _tell_sector(normed_own)
     columns = normed_rows
     gate_value = jnp.dot(
         columns,

time: 491 us -> 462 us (0.941)
  waiting for transfers between devices: 335 us -> 292 us
  local copies, waits for them, and re-layouts: 7.45 us -> 19 us
    all_gather x1, waiting for transfers between devices: 70.8 us -> 24.3 us  [body(): lax.all_gather(mixer_gate_weight, 'sp', axis=0, tiled=True)]
    ppermute x0 -> x3, waiting for transfers between devices: none -> 34.6 us  [_tell_sector(): small = jax.lax.ppermute(small, axis_name='tp', perm=block_last)]
    all_gather x1 -> x0, waiting for transfers between devices: 28.1 us -> none  [body(): normed_rows = lax.all_gather(normed_own, 'tp', axis=1, tiled=True)]
    unnamed x22 -> x30, local copies, waits for them, and re-layouts: 0.87 us -> 12.5 us
  transfers between devices with their start and end apart: 7 -> 9, of which waited for: 6 -> 8; matrix products, arithmetic and copies ran while one was open for 4% -> 7% of each run, Pallas kernels for 0% -> 0%
where the time goes in v1:
time: 462 us; the launch traced here: 461 us
  waiting for transfers between devices  292 us (63%)
  blocking collectives  70.2 us (15%)
  matrix products  42.2 us (9%)
  other arithmetic  22.8 us (5%)
  local copies, waits for them, and re-layouts  19 us (4%)
  between operations  14.3 us (3%)
    all_gather x1, waiting for transfers between devices, body(): lax.all_gather(mixer_down_weight, 'sp', axis=1, tiled=True)  86.9 us
    all_gather x1, waiting for transfers between devices, body(): lax.all_gather(mixer_up_weight, 'sp', axis=0, tiled=True)  76.5 us
    all_gather x2, blocking collectives, carried_in(): pieces = jax.tree.map(lambda part: lax.all_gather(part, axis), value)  41.2 us
    reduce_scatter x1, waiting for transfers between devices, body(): lax.psum_scatter(down_terms.astype(jnp.bfloat16), 'tp', scatter_dimension...  36.1 us
    ppermute x3, waiting for transfers between devices, _tell_sector(): small = jax.lax.ppermute(small, axis_name='tp', perm=block_last)  34.6 us
    reduce_scatter x1, waiting for transfers between devices, body(): lax.psum_scatter(lax.dot_general(columns, gated, (((0,), (1,)), ((), ()))...  31.7 us
    all_gather x1, waiting for transfers between devices, body(): lax.all_gather(mixer_gate_weight, 'sp', axis=0, tiled=True)  24.3 us
    unnamed x1, blocking collectives  17.6 us
  transfers between devices with their start and end apart: 9, of which 8 were waited for; matrix products, arithmetic and copies ran while one was open for 7% of the time, Pallas kernels for 0%

profile of v1, /device:TPU:0, one launch (start us, length us, event | category | flops | bytes accessed | tf_op | source)
XLA Modules:
  0.0 460.7 jit_solution(16166256015986355159)
XLA Ops:
  9.9 1.4 copy.54
  11.4 2.8 fusion.37
  15.7 22.4 %all-gather.3 = f32[8,1,2]{2,1,0:T(1,128)S(1)} all-gather(f32[1,1,2]{2,1,0:T(1,128)S(1)} %fusion.66), channel_id=1, replica_groups=mesh['sp'=8,'tp'=4] {'sp'}, dimensions={0}, use_global_device_ids=true | all-gather | bytes 72 | tf_op jit(solution)/shard_map/all_gather | solution.py:15
  38.1 17.6 %all-reduce = f32[16]{0:T(128)S(1)} all-reduce(f32[16]{0:T(128)S(1)} %dynamic-update-slice), channel_id=2, replica_groups=mesh['sp'=8,'tp'=4] {'sp'}, use_global_device_ids=true, to_apply=%add | all-reduce | flops 16 | bytes 128
  57.2 18.8 %all-gather.4 = f32[8,2,128]{2,1,0:T(2,128)S(1)} all-gather(f32[1,2,128]{2,1,0:T(2,128)S(1)} %add_bitcast_fusion.1), channel_id=4, replica_groups=mesh['sp'=8,'tp'=4] {'sp'}, dimensions={0}, use_global_device_ids=true | all-gather | bytes 9216 | tf_op jit(solution)/shard_map/all_gather | solution.py:15
  77.2 8.3 %while.20 = (s32[]{:T(128)}, f32[2]{0:T(128)S(1)}, f32[2,256,128]{2,1,0:T(8,128)S(1)}, f32[2,128]{1,0:T(2,128)S(1)}, f32[2]{0:T(128)S(1)}, /*index=5*/s32[]{:T(1...) while((s32[]{:T(128)}, f32[2]{0:T(128)S(1)}, ...), condition=%wide.region_4.5_spmd.clone, body=%wide.region_3.4_spmd.clone.sunk | while | flops 328984 | bytes 789781 | solution.py:24
  85.7 3.0 fusion.15
  89.5 1.5 fusion.44
  91.1 2.4 fusion.79
  93.8 1.5 fusion.33
  95.4 3.0 copy.47
  98.4 4.9 %fusion.8 = bf16[2048,768]{0,1:T(8,128)(2,1)} fusion(bf16[512,2048]{1,0:T(8,128)(2,1)S(1)} %copy-done, f32[768,512]{1,0:T(8,128)} %copy.47, bf16[768,512]{1,0:T(8,128)(2,1)S(1)} %copy-done.8), kind=kOutput, calls=%fused_computation.23 | convolution fusion | flops 1614544896 | bytes 7602176 | tf_op jit(solution)/shard_map/dot_general | solution.py:149
  106.8 31.7 %reduce-scatter.3.cloned.1.call-done = bf16[512,768]{0,1:T(8,128)(2,1)} async-done(((bf16[2048,768]{0,1:T(8,128)(2,1)}), bf16[512,768]{0,1:T(8,128)(2,1)}) %reduce-scatter.3.cloned.1.call-update) | async-done | bytes 786448 | tf_op jit(solution)/shard_map/reduce_scatter | solution.py:148
  138.5 1.4 fusion.20
  139.8 5.8 %psum.14 = f32[768]{0:T(1024)S(1)} all-reduce(f32[768]{0:T(1024)S(1)} %fusion.20), channel_id=1, replica_groups=mesh['sp'=8,'tp'=4] {'tp'}, use_global_device_ids=true, to_apply=%region_11.12 | all-reduce | flops 768 | bytes 6144 | tf_op jit(solution)/shard_map/psum | solution.py:159
  145.6 1.7 fusion.24
  147.5 5.7 %psum.15 = f32[768]{0:T(1024)S(1)} all-reduce(f32[768]{0:T(1024)S(1)} %fusion.25), channel_id=1, replica_groups=mesh['sp'=8,'tp'=4] {'tp'}, use_global_device_ids=true, to_apply=%region_13.14 | all-reduce | flops 768 | bytes 6144 | tf_op jit(solution)/shard_map/psum | solution.py:168
  153.5 11.4 %collective-permute-done = bf16[768,512]{1,0:T(8,128)(2,1)S(1)} collective-permute-done((bf16[768,512]{1,0:T(8,128)(2,1)S(1)}, bf16[768,512]{1,0:T(8,128)(2,1)S(1)}, u32[]{:S(2)}, u32[]{:S(2)}) %collective-permute-start) | collective-permute-done | bytes 786464 | tf_op jit(solution)/shard_map/ppermute | solution.py:180
  165.8 11.5 %collective-permute-done.1 = bf16[768,512]{1,0:T(8,128)(2,1)} collective-permute-done((bf16[768,512]{1,0:T(8,128)(2,1)S(1)}, bf16[768,512]{1,0:T(8,128)(2,1)}, u32[]{:S(2)}, u32[]{:S(2)}) %collective-permute-start.1) | collective-permute-done | bytes 786464 | tf_op jit(solution)/shard_map/ppermute | solution.py:180
  177.4 11.7 %collective-permute-done.2 = bf16[768,512]{1,0:T(8,128)(2,1)} collective-permute-done((bf16[768,512]{1,0:T(8,128)(2,1)}, bf16[768,512]{1,0:T(8,128)(2,1)}, u32[]{:S(2)}, u32[]{:S(2)}) %collective-permute-start.2) | collective-permute-done | bytes 786464 | tf_op jit(solution)/shard_map/ppermute | solution.py:180
  189.1 2.2 constant_dynamic-update-slice_fusion.7
  191.2 2.2 constant_dynamic-update-slice_fusion.6
  194.5 1.3 constant_dynamic-update-slice_fusion.4
  195.8 2.1 constant_dynamic-update-slice_fusion.3
  197.9 2.1 constant_dynamic-update-slice_fusion.2
  202.3 24.3 %all-gather.10.cloned.1.call-done = bf16[2048,1280]{1,0:T(8,128)(2,1)} async-done(((bf16[256,1280]{1,0:T(8,128)(2,1)}), bf16[2048,1280]{1,0:T(8,128)(2,1)}) %all-gather.10.cloned.1.call-update) | async-done | bytes 5242896 | tf_op jit(solution)/shard_map/all_gather | solution.py:190
  226.6 9.6 %fusion.11 = f32[768,1280]{1,0:T(8,128)} fusion(bf16[2048,1280]{1,0:T(8,128)(2,1)} %all-gather.10.cloned.1.call-done, bf16[768,4096]{1,0:T(8,128)(2,1)} %constant_dynamic-update-slice_fusion, s32[]{:T(128)S(6)} %select_n.95), kind=kOutput, calls=%fused_computation.26 | convolution fusion | flops 4026531840 | bytes 12320772 | tf_op jit(solution)/shard_map/dot_general | solution.py:188
  236.2 76.5 %all-gather.12.cloned.1.call-done = bf16[2048,1280]{1,0:T(8,128)(2,1)} async-done(((bf16[256,1280]{1,0:T(8,128)(2,1)}), bf16[2048,1280]{1,0:T(8,128)(2,1)}) %all-gather.12.cloned.1.call-update) | async-done | bytes 5242896 | tf_op jit(solution)/shard_map/all_gather | solution.py:195
  312.7 86.9 %all-gather.14.cloned.1.call-done = bf16[1280,2048]{1,0:T(8,128)(2,1)} async-done(((bf16[1280,256]{1,0:T(8,128)(2,1)}), bf16[1280,2048]{1,0:T(8,128)(2,1)}) %all-gather.14.cloned.1.call-update) | async-done | bytes 5242896 | tf_op jit(solution)/shard_map/all_gather | solution.py:201
  399.6 16.0 %convolution_convert_fusion.1 = bf16[768,2048]{1,0:T(8,128)(2,1)} fusion(bf16[1280,2048]{1,0:T(8,128)(2,1)} %all-gather.14.cloned.1.call-done, f32[768,1280]{1,0:T(8,128)} %fusion.11, bf16[2048,1280]{1,0:T(8,128)(2,1)} %all-gather.12.cloned.1.call-done, bf16[768,4096]{1,0:T(8,128)(2,1)} %constant_dynamic-update-slice_fusion, s32[]{:T(128)S(6)} %select_n.95), kind=kOutput, calls=%fused_computation.22 | convolution fusion | flops 8060534784 | bytes 20709380 | tf_op jit(solution)/shard_map/dot_general | solution.py:199
  415.6 36.1 %reduce-scatter.5.cloned.1.call-done = bf16[768,512]{1,0:T(8,128)(2,1)} async-done(((bf16[768,2048]{1,0:T(8,128)(2,1)}), bf16[768,512]{1,0:T(8,128)(2,1)}) %reduce-scatter.5.cloned.1.call-update) | async-done | bytes 786448 | tf_op jit(solution)/shard_map/reduce_scatter | solution.py:204
  451.6 2.2 fusion.28
  (109 shorter events, 24.7 us)
Async XLA Ops:
  6.5 91.8 %copy-start = (bf16[512,2048]{1,0:T(8,128)(2,1)S(1)}, bf16[512,2048]{1,0:T(8,128)(2,1)}, u32[]{:S(2)}) copy-start(bf16[512,2048]{1,0:T(8,128)(2,1)} %param.26) | copy-start | bytes 6291460
  6.5 7.8 %copy-start.9 = (u32[32]{0:T(128)S(1)}, u32[32]{0:T(128)}, u32[]{:S(2)}) copy-start(u32[32]{0:T(128)} %constant.99) | copy-start | bytes 388
  6.5 69.7 %copy-start.6 = (f32[768,2]{0,1:T(2,128)S(1)}, f32[768,2]{0,1:T(2,128)}, u32[]{:S(2)}) copy-start(f32[768,2]{0,1:T(2,128)} %param.22) | copy-start | bytes 18436
  6.5 49.2 %copy-start.7 = (f32[512]{0:T(512)S(1)}, f32[512]{0:T(512)}, u32[]{:S(2)}) copy-start(f32[512]{0:T(512)} %param.25) | copy-start | bytes 6148
  6.5 70.7 %all-gather.16.cloned.1.call-start = ((), (), s32[]{:S(2)}) async-start(), calls=%async_computation.7 | async-start | bytes 2359296 | tf_op jit(solution)/shard_map/all_gather | solution.py:15
  11.3 26.8 %copy-start.3 = (bf16[768,512]{0,1:T(8,128)(2,1)}, bf16[768,512]{0,1:T(8,128)(2,1)S(1)}, u32[]{:S(2)}) copy-start(bf16[768,512]{0,1:T(8,128)(2,1)S(1)} %copy.54) | copy-start | bytes 2359300
  14.2 71.4 %copy-start.5 = (bf16[768,256]{1,0:T(8,128)(2,1)S(1)}, bf16[768,256]{1,0:T(8,128)(2,1)}, u32[]{:S(2)}) copy-start(bf16[768,256]{1,0:T(8,128)(2,1)} %param.18) | copy-start | bytes 1179652
  14.3 124.2 %reduce-scatter.3.cloned.1.call-start = ((), (), s32[]{:S(2)}) async-start(), calls=%async_computation.2 | async-start | bytes 3932160 | tf_op jit(solution)/shard_map/reduce_scatter | solution.py:148
  85.7 5.4 %copy-start.4 = (bf16[768,512]{0,1:T(8,128)(2,1)S(1)}, bf16[768,512]{0,1:T(8,128)(2,1)}, u32[]{:S(2)}) copy-start(bf16[768,512]{0,1:T(8,128)(2,1)} %copy-done.3) | copy-start | bytes 2359300
  93.8 4.6 copy-start.8
  103.3 123.3 %all-gather.10.cloned.1.call-start = ((), (), s32[]{:S(2)}) async-start(), calls=%async_computation.3 | async-start | bytes 5898240 | tf_op jit(solution)/shard_map/all_gather | solution.py:190
  104.0 208.7 %all-gather.12.cloned.1.call-start = ((), (), s32[]{:S(2)}) async-start(), calls=%async_computation.4 | async-start | bytes 5898240 | tf_op jit(solution)/shard_map/all_gather | solution.py:195
  104.6 295.0 %all-gather.14.cloned.1.call-start = ((), (), s32[]{:S(2)}) async-start(), calls=%async_computation.5 | async-start | bytes 5898240 | tf_op jit(solution)/shard_map/all_gather | solution.py:201
  105.2 346.4 %reduce-scatter.5.cloned.1.call-start = ((), (), s32[]{:S(2)}) async-start(), calls=%async_computation.6 | async-start | bytes 3932160 | tf_op jit(solution)/shard_map/reduce_scatter | solution.py:204
  153.5 11.5 %collective-permute-start = (bf16[768,512]{1,0:T(8,128)(2,1)S(1)}, bf16[768,512]{1,0:T(8,128)(2,1)S(1)}, u32[]{:S(2)}, u32[]{:S(2)}) collective-permute-start(bf16[768,512]{1,0:T(8,128)(2,1)S(1)} %fusion.27), channel_id=1, source_target_pairs={{0,1},{1,2},{2,3},{3,0},{4,5},{5,6},{6,7},{7,4},{8,9},{9,10},{10,1... | collective-permute-start | bytes 2359304 | tf_op jit(solution)/shard_map/ppermute | solution.py:180
  164.9 0.9 copy-start.1
  165.8 11.5 %collective-permute-start.1 = (bf16[768,512]{1,0:T(8,128)(2,1)S(1)}, bf16[768,512]{1,0:T(8,128)(2,1)}, u32[]{:S(2)}, u32[]{:S(2)}) collective-permute-start(bf16[768,512]{1,0:T(8,128)(2,1)S(1)} %collective-permute-done), channel_id=1, source_target_pairs={{0,1},{1,2},{2,3},{3,0},{4,5},{5,6},{6,7},{7,4},{8,9},{9,10},{10,1... | collective-permute-start | bytes 2359304 | tf_op jit(solution)/shard_map/ppermute | solution.py:180
  177.3 11.7 %collective-permute-start.2 = (bf16[768,512]{1,0:T(8,128)(2,1)}, bf16[768,512]{1,0:T(8,128)(2,1)}, u32[]{:S(2)}, u32[]{:S(2)}) collective-permute-start(bf16[768,512]{1,0:T(8,128)(2,1)} %collective-permute-done.1), channel_id=1, source_target_pairs={{0,1},{1,2},{2,3},{3,0},{4,5},{5,6},{6,7},{7,4},{8,9},{9,10},{10,1... | collective-permute-start | bytes 2359304 | tf_op jit(solution)/shard_map/ppermute | solution.py:180
  177.3 16.1 %copy-start.2 = (bf16[768,512]{1,0:T(8,128)(2,1)S(1)}, bf16[768,512]{1,0:T(8,128)(2,1)}, u32[]{:S(2)}) copy-start(bf16[768,512]{1,0:T(8,128)(2,1)} %copy-done.1) | copy-start | bytes 2359300
Sparse Core Ops, SparseCore 0:
  14.4 52.0 all-gather.15
  103.4 34.9 reduce-scatter.2
  140.6 85.8 all-gather.9
  228.6 84.0 all-gather.11
  314.6 84.9 all-gather.13
  415.7 35.9 reduce-scatter.4
